TPU v7x, 32 devices: a whole 2x2x4 slice. The times are simulated.
32 devices in a mesh: fs: 8 (over z, y), tp: 4 (over x, core).
Axes of the slice: x: 2, y: 2, z: 4, core: 2. Of those that a mesh axis runs over, the one named last changes fastest.
Arguments:
- tokens: bfloat16 [3072, 2048], P('tp'), may hold values from -6 to 6
- norm_gain: float32 [2048], P('fs'), may hold values from 0.1 to 1.9
- gate_weight: float32 [4, 2048, 8192], P(None, 'fs', 'tp'), may hold values from -0.125 to 0.125
- up_weight: float32 [4, 2048, 8192], P(None, 'fs', 'tp'), may hold values from -0.125 to 0.125
- down_weight: float32 [4, 8192, 2048], P(None, 'fs', 'tp'), may hold values from -0.0625 to 0.0625
- routes: int32 [3072, 2], P('tp'), may hold values from 0 to 3, all different within a row; in each aligned block of 768 rows (0 to 767, 768 to 1535, ...) at most 480 rows name the same one
- route_logit: float32 [3072, 2], P('tp'), may hold values from -6 to 6
Outputs:
- gate_out: bfloat16 [4, 2048, 8192], P(None, None, 'fs')
- up_out: bfloat16 [4, 2048, 8192], P(None, None, 'fs')
- down_out: bfloat16 [4, 8192, 2048], P(None, 'fs')
- mixed: bfloat16 [3072, 2048], P(('tp', 'fs'))
Inputs may be any that keep to these rules, and one draw needn't show every extreme that they name: `routes`: the two experts of a token differ. In each aligned block of 768 tokens (the tokens of one request group) every expert is named by at most 480 tokens, a bound that some block reaches.
All inputs are finite; a program needn't handle non-finite values.
Results may differ from a plain program's by a relative error of at most 0.0082.
Values may be sent and summed in bfloat16 or wider, within the bound.
No kernel may reach another device: no remote copies, remote signals or barrier semaphores. Data moves between devices by JAX's collectives and lax.ppermute only.
A program may use at most 192 MiB of HBM per device.

v0:
```python
import jax
import jax.numpy as jnp
from jax import lax
from jax.sharding import PartitionSpec as P

EPS = 0.5


def shards(tokens, norm_gain, gate_weight, up_weight, down_weight, routes, route_logit):
    gain_col = norm_gain[None, :, None]
    gate_part = (gate_weight * gain_col).astype(jnp.bfloat16)
    up_part = (up_weight * gain_col).astype(jnp.bfloat16)
    down_part = down_weight.astype(jnp.bfloat16)
    gate_one, up_one = (
        lax.all_to_all(gate_part, "tp", split_axis=0, concat_axis=2, tiled=True),
        lax.all_to_all(up_part, "tp", split_axis=0, concat_axis=2, tiled=True),
    )
    gate_mine, up_mine = (
        lax.all_to_all(gate_one, "fs", split_axis=2, concat_axis=1, tiled=True),
        lax.all_to_all(up_one, "fs", split_axis=2, concat_axis=1, tiled=True),
    )
    gate_out, up_out = (
        lax.all_gather(gate_mine, "tp", axis=0, tiled=True),
        lax.all_gather(up_mine, "tp", axis=0, tiled=True),
    )
    down_out = lax.all_gather(down_part, "tp", axis=2, tiled=True)
    total_rows = tokens.shape[0]
    width = tokens.shape[1]
    experts = gate_out.shape[0]
    capacity = total_rows * 5 // 8
    floats = tokens.astype(jnp.float32)
    normed = (floats * lax.rsqrt(jnp.mean(floats * floats, axis=1, keepdims=True) + EPS)).astype(
        jnp.bfloat16
    )
    first_share = jax.nn.sigmoid(route_logit[:, 0] - route_logit[:, 1])
    shares = jnp.stack([first_share, 1.0 - first_share], axis=1)
    chosen = (routes[:, :, None] == jnp.arange(experts, dtype=jnp.int32)[None, None, :]).astype(
        jnp.int32
    )
    counts = jnp.sum(chosen, axis=1)
    before = jnp.cumsum(counts, axis=0) - counts
    slot_index = jnp.sum(chosen * before[:, None, :], axis=2)
    flat_slot = routes * capacity + slot_index
    row_ids = jnp.repeat(jnp.arange(total_rows, dtype=jnp.int32), 2)
    table = (
        jnp.full((experts * capacity,), total_rows, jnp.int32)
        .at[flat_slot.reshape(-1)]
        .set(row_ids)
    )
    gathered = jnp.take(normed, table, axis=0, mode="fill", fill_value=0).reshape(
        experts, capacity, width
    )
    gate_val = jnp.einsum("ecd,edf->ecf", gathered, gate_out, preferred_element_type=jnp.float32)
    up_val = jnp.einsum("ecd,edf->ecf", gathered, up_out, preferred_element_type=jnp.float32)
    hidden = (jax.nn.silu(gate_val) * up_val).astype(jnp.bfloat16)
    results = jnp.einsum("ecf,efd->ecd", hidden, down_out, preferred_element_type=jnp.float32)
    flat_rows = results.reshape(experts * capacity, width)
    first_rows = jnp.take(flat_rows, flat_slot[:, 0], axis=0)
    second_rows = jnp.take(flat_rows, flat_slot[:, 1], axis=0)
    mixed = lax.psum_scatter(
        shares[:, 0:1] * first_rows + shares[:, 1:2] * second_rows,
        "fs",
        scatter_dimension=0,
        tiled=True,
    )
    return (gate_out, up_out, down_out, mixed.astype(jnp.bfloat16))


def solution(mesh):
    return jax.shard_map(
        shards,
        mesh=mesh,
        in_specs=(
            P("tp", None),
            P("fs"),
            P(None, "fs", "tp"),
            P(None, "fs", "tp"),
            P(None, "fs", "tp"),
            P("tp", None),
            P("tp", None),
        ),
        out_specs=(
            P(None, None, "fs"),
            P(None, None, "fs"),
            P(None, "fs", None),
            P(("tp", "fs"), None),
        ),
        check_vma=False,
    )
```

profile of v0, /device:TPU:0, one launch (start us, length us, event | category | flops | bytes accessed | tf_op | source)
XLA Modules:
  0.0 959.0 jit_solution(9687158230475078291)
XLA Ops:
  7.2 0.0 all-gather.6.cloned.1.call-start
  7.2 8.7 copy.43
  15.9 0.0 copy-start.3
  15.9 8.7 copy.46
  24.6 0.0 copy-done.3
  24.6 10.7 %multiply_convert_fusion = (bf16[4,256,2048]{1,2,0:T(8,128)(2,1)}, bf16[4,256,2048]{1,2,0:T(8,128)(2,1)}) fusion(f32[4,256,2048]{1,2,0:T(8,128)} %copy.46, f32[256]{0:T(256)S(1)} %copy-done.3, f32[4,256,2048]{1,2,0:T(8,128)} %copy.43), kind=kLoop, calls=%fused_computation.4 | loop fusion | flops 8388608 | bytes 25166848 | tf_op jit(solution)/shard_map/convert_element_type | solution.py:12
  35.3 52.6 %all_to_all.72 = bf16[4,256,2048]{1,2,0:T(8,128)(2,1)S(1)} all-to-all(bf16[4,256,2048]{1,2,0:T(8,128)(2,1)} %get-tuple-element.9), channel_id=1, replica_groups=mesh['fs'=8,'tp'=4] {'tp'}, dimensions={0} | all-to-all | bytes 8388608 | tf_op jit(solution)/shard_map/all_to_all | solution.py:16
  87.9 49.3 %copy.56 = bf16[1,256,8192]{1,0,2:T(2,128)(2,1)} copy(bf16[1,256,8192]{1,2,0:T(8,128)(2,1)S(1)} %bitcast.49) | data formatting | bytes 8388608 | tf_op jit(solution)/shard_map/all_to_all | solution.py:16
  137.2 0.5 broadcast.78
  137.7 43.5 %reduce.13 = bf16[8192,256]{1,0:T(8,128)(2,1)} reduce(bf16[8192,1,256]{2,1,0:T(2,128)(2,1)} %bitcast.45, bf16[]{:T(256)} %broadcast.78), dimensions={1}, to_apply=%bitcast.40.reduce_sub_computation | reduce | bytes 8388610
  181.2 6.9 reshape.137
  188.2 99.8 %all_to_all.73 = bf16[8,2,131072]{2,1,0:T(2,128)(2,1)} all-to-all(bf16[8,2,131072]{2,1,0:T(2,128)(2,1)} %reshape.137), channel_id=1, replica_groups=mesh['fs'=8,'tp'=4] {'fs'}, dimensions={0} | all-to-all | bytes 8388608 | tf_op jit(solution)/shard_map/all_to_all | solution.py:20
  288.0 8.7 reshape.138
  296.7 6.1 copy.51
  302.8 6.4 copy.48
  309.3 0.0 all-gather.6.cloned.1.call-update
  309.3 0.0 all-gather.8.cloned.1.call-start
  309.3 6.0 convert_element_type.26
  315.4 0.0 all-gather.8.cloned.1.call-update
  315.4 0.0 all-gather.4.cloned.1.call-start
  315.4 97.4 %all_to_all.74 = bf16[4,256,2048]{1,2,0:T(8,128)(2,1)S(1)} all-to-all(bf16[4,256,2048]{1,2,0:T(8,128)(2,1)} %get-tuple-element.10), channel_id=1, replica_groups=mesh['fs'=8,'tp'=4] {'tp'}, dimensions={0} | all-to-all | bytes 8388608 | tf_op jit(solution)/shard_map/all_to_all | solution.py:15
  412.8 49.3 %copy.57 = bf16[1,256,8192]{1,0,2:T(2,128)(2,1)} copy(bf16[1,256,8192]{1,2,0:T(8,128)(2,1)S(1)} %bitcast.51) | data formatting | bytes 8388608 | tf_op jit(solution)/shard_map/all_to_all | solution.py:15
  462.2 43.5 %reduce.12 = bf16[8192,256]{1,0:T(8,128)(2,1)} reduce(bf16[8192,1,256]{2,1,0:T(2,128)(2,1)} %bitcast.46, bf16[]{:T(256)} %broadcast.78), dimensions={1}, to_apply=%bitcast.41.reduce_sub_computation | reduce | bytes 8388610
  505.7 7.0 reshape.135
  512.7 97.7 %all_to_all.75 = bf16[8,2,131072]{2,1,0:T(2,128)(2,1)} all-to-all(bf16[8,2,131072]{2,1,0:T(2,128)(2,1)} %reshape.135), channel_id=1, replica_groups=mesh['fs'=8,'tp'=4] {'fs'}, dimensions={0} | all-to-all | bytes 8388608 | tf_op jit(solution)/shard_map/all_to_all | solution.py:19
  610.4 8.7 reshape.136
  619.1 6.1 copy.50
  625.2 0.0 copy-start.1
  625.2 6.6 copy.45
  631.8 0.0 all-gather.4.cloned.1.call-update
  631.8 0.0 reduce-scatter.2.cloned.1.call-start
  631.9 0.0 copy-done.1
  631.9 1.1 reduce-window.6
  633.1 0.2 slice_reduce_fusion
  633.3 0.2 reduce-window.9
  633.5 0.1 add_bitcast_fusion
  633.6 0.2 copy.49
  633.8 0.3 reshape.85
  634.1 0.8 reshape.116
  634.9 6.3 scatter_custom_fusion
  641.3 0.1 broadcast_in_dim.37
  641.4 0.0 copy-done
  641.4 0.7 fusion.2
  642.1 2.8 fusion.3
  644.9 0.0 copy-start.2
  644.9 8.9 gather_fusion
  653.9 0.0 copy-done.2
  653.9 0.0 all-gather.6.cloned.1.call-done
  654.0 16.3 %fusion = f32[4,480,1024]{2,1,0:T(8,128)} fusion(bf16[4,2048,1024]{2,1,0:T(8,128)(2,1)} %all-gather.6.cloned.1.call-done, bf16[4,480,2048]{2,1,0:T(8,128)(2,1)} %bitcast.57, pred[4,480]{1,0:T(4,128)(4,1)S(1)} %broadcast_in_dim.37), kind=kOutput, calls=%fused_computation.10 | convolution fusion | flops 8056995840 | bytes 32507776 | tf_op jit(solution)/shard_map/ecd,edf->ecf/dot_general | solution.py:54
  670.2 65.7 %all-gather.4.cloned.1.call-done = bf16[4,2048,1024]{2,1,0:T(8,128)(2,1)} async-done(((bf16[1,2048,1024]{2,1,0:T(8,128)(2,1)}), bf16[4,2048,1024]{2,1,0:T(8,128)(2,1)}) %all-gather.4.cloned.1.call-update) | async-done | bytes 16777232 | tf_op jit(solution)/shard_map/all_gather | solution.py:23
  735.9 27.2 %fusion.7 = f32[4,480,2048]{2,1,0:T(8,128)} fusion(bf16[4,1024,2048]{2,1,0:T(8,128)(2,1)} %all-gather.8.cloned.1.call-done, f32[4,480,1024]{2,1,0:T(8,128)} %fusion, bf16[4,2048,1024]{2,1,0:T(8,128)(2,1)} %all-gather.4.cloned.1.call-done, bf16[4,480,2048]{2,1,0:T(8,128)(2,1)} %bitcast.58, pred[4,480]{1,0:T(4,128)(4,1)S(1)} %broadcast_in_dim.37), kind=kOutput, calls=%fused_computation.19 | convolution fusion | flops 16121856000 | bytes 65013632 | tf_op jit(solution)/shard_map/ecf,efd->ecd/dot_general | solution.py:56
  763.1 12.7 %gather_fusion.1 = f32[768,2048]{1,0:T(8,128)} fusion(f32[1920,2048]{1,0:T(8,128)} %bitcast.43, s32[1024]{0:T(1024)S(1)} %pad_clamp_fusion.2), kind=kCustom, calls=%fused_computation.clone | custom fusion | bytes 12585984 | tf_op jit(solution)/shard_map/jit(_take)/gather | solution.py:58
  775.8 12.7 %gather_fusion.2 = f32[768,2048]{1,0:T(8,128)} fusion(f32[1920,2048]{1,0:T(8,128)} %bitcast.44, s32[1024]{0:T(1024)S(1)} %pad_clamp_fusion.1), kind=kCustom, calls=%fused_computation.1.clone | custom fusion | bytes 12585984 | tf_op jit(solution)/shard_map/jit(_take)/gather | solution.py:59
  788.5 7.2 fusion.4
  795.7 0.0 reduce-scatter.2.cloned.1.call-update
  795.7 118.2 %reduce-scatter.2.cloned.1.call-done = f32[96,2048]{1,0:T(8,128)} async-done(((f32[768,2048]{1,0:T(8,128)}), f32[96,2048]{1,0:T(8,128)}) %reduce-scatter.2.cloned.1.call-update) | async-done | bytes 786448 | tf_op jit(solution)/shard_map/reduce_scatter | solution.py:60
  913.9 1.9 convert_element_type.31
  915.8 15.2 %copy.61 = bf16[4,2048,1024]{2,1,0:T(8,128)(2,1)} copy(bf16[4,2048,1024]{2,1,0:T(8,128)(2,1)} %all-gather.4.cloned.1.call-done) | data formatting | bytes 33554432
  931.1 15.2 %copy.62 = bf16[4,2048,1024]{2,1,0:T(8,128)(2,1)} copy(bf16[4,2048,1024]{2,1,0:T(8,128)(2,1)} %all-gather.6.cloned.1.call-done) | data formatting | bytes 33554432
  946.3 0.0 slice-done
  946.3 0.0 slice-done.1
  946.3 0.0 slice-done.2
  946.3 0.0 slice-done.3
  946.3 6.2 copy.63
  (24 shorter events, 0.3 us)
Async XLA Ops:
  7.2 646.8 %all-gather.6.cloned.1.call-start = ((), (), s32[]{:S(2)}) async-start(), calls=%async_computation.6 | async-start | bytes 20971520 | tf_op jit(solution)/shard_map/all_gather | solution.py:24
  15.9 8.7 copy-start.3
  309.3 360.9 %all-gather.8.cloned.1.call-start = ((), (), s32[]{:S(2)}) async-start(), calls=%async_computation.7 | async-start | bytes 20971520 | tf_op jit(solution)/shard_map/all_gather | solution.py:26
  315.4 420.5 %all-gather.4.cloned.1.call-start = ((), (), s32[]{:S(2)}) async-start(), calls=%async_computation.5 | async-start | bytes 20971520 | tf_op jit(solution)/shard_map/all_gather | solution.py:23
  625.2 6.7 copy-start.1
  625.2 16.2 %copy-start = (bf16[768,2048]{1,0:T(8,128)(2,1)S(1)}, bf16[768,2048]{1,0:T(8,128)(2,1)}, u32[]{:S(2)}) copy-start(bf16[768,2048]{1,0:T(8,128)(2,1)} %param.9) | copy-start | bytes 9437188
  631.8 282.1 %reduce-scatter.2.cloned.1.call-start = ((), (), s32[]{:S(2)}) async-start(), calls=%async_computation.8 | async-start | bytes 7077888 | tf_op jit(solution)/shard_map/reduce_scatter | solution.py:60
  644.9 8.9 copy-start.2
  915.8 30.5 %slice-start = ((s8[16777216]{0:T(1024)(128)(4,1)}), s8[4194304]{0:T(1024)(128)(4,1)S(1)}, s32[]{:S(2)}) async-start(s8[16777216]{0:T(1024)(128)(4,1)} %bitcast.53), calls=%async_computation.9 | async-start | bytes 8388608
  915.8 30.5 %slice-start.1 = ((s8[16777216]{0:T(1024)(128)(4,1)}), s8[4194304]{0:T(1024)(128)(4,1)S(1)}, s32[]{:S(2)}) async-start(s8[16777216]{0:T(1024)(128)(4,1)} %bitcast.53), calls=%async_computation.10 | async-start | bytes 8388608
  931.1 15.2 %slice-start.2 = ((s8[16777216]{0:T(1024)(128)(4,1)}), s8[4194304]{0:T(1024)(128)(4,1)S(1)}, s32[]{:S(2)}) async-start(s8[16777216]{0:T(1024)(128)(4,1)} %bitcast.53), calls=%async_computation.11 | async-start | bytes 8388608
  931.1 15.2 %slice-start.3 = ((s8[16777216]{0:T(1024)(128)(4,1)}), s8[4194304]{0:T(1024)(128)(4,1)S(1)}, s32[]{:S(2)}) async-start(s8[16777216]{0:T(1024)(128)(4,1)} %bitcast.53), calls=%async_computation.12 | async-start | bytes 8388608
Sparse Core Ops, SparseCore 0:
  309.4 148.9 all-gather.5
  460.0 104.8 all-gather.7
  631.9 103.9 all-gather.3
  795.8 118.0 reduce-scatter.1
where the time goes:
time: 961 us; the launch traced here: 959 us
  blocking collectives  347 us (36%)
  local copies, waits for them, and re-layouts  252 us (26%)
  waiting for transfers between devices  184 us (19%)
  other arithmetic  118 us (12%)
  matrix products  43.5 us (5%)
  between operations  14 us (1%)
    reduce_scatter x1, waiting for transfers between devices, shards(): lax.psum_scatter(shares[:, 0:1] * first_rows + shares[:, 1:2] * second_ro...  118 us
    all_to_all x1, blocking collectives, shards(): lax.all_to_all(up_one, 'fs', split_axis=2, concat_axis=1, tiled=True)  99.8 us
    unnamed x28, local copies, waits for them, and re-layouts  98.2 us
    all_to_all x1, blocking collectives, shards(): lax.all_to_all(gate_one, 'fs', split_axis=2, concat_axis=1, tiled=True)  97.7 us
    all_to_all x1, blocking collectives, shards(): lax.all_to_all(gate_part, 'tp', split_axis=0, concat_axis=2, tiled=True)  97.4 us
    unnamed x4, other arithmetic  87.2 us
    all_gather x1, waiting for transfers between devices, shards(): lax.all_gather(gate_mine, 'tp', axis=0, tiled=True)  65.7 us
    all_to_all x1, blocking collectives, shards(): lax.all_to_all(up_part, 'tp', split_axis=0, concat_axis=2, tiled=True)  52.6 us
  transfers between devices with their start and end apart: 4, of which 2 were waited for; matrix products, arithmetic and copies ran while one was open for 17% of the time, Pallas kernels for 0%

commit v1 on v0

--- a/solution.py
+++ b/solution.py
@@ -1,9 +1,322 @@
+import functools
+
 import jax
 import jax.numpy as jnp
 from jax import lax
+from jax.experimental import pallas as pl
+from jax.experimental.pallas import tpu as pltpu
 from jax.sharding import PartitionSpec as P
 
+
 EPS = 0.5
+ANY = pl.BlockSpec(memory_space=pl.ANY)
+SMEM = pl.BlockSpec(memory_space=pltpu.SMEM)
+VMEM = pl.BlockSpec(memory_space=pltpu.VMEM)
+
+
+def cast_whole(gate_ref, up_ref, gain_ref, own_ref):
+    gain = gain_ref[...]
+    own_ref[0, 0] = (gate_ref[0] * gain).astype(jnp.bfloat16)
+    own_ref[0, 1] = (up_ref[0] * gain).astype(jnp.bfloat16)
+
+
+def cast_halves(where_ref, gate_ref, up_ref, gain_ref, keep_ref, send_ref):
+    half = keep_ref.shape[2]
+    x = where_ref[0]
+    for out_ref, at in ((keep_ref, x), (send_ref, 1 - x)):
+        rows = pl.ds(pl.multiple_of(at * half, half), half)
+        gain = gain_ref[rows, :]
+        out_ref[0, 0] = (gate_ref[0, rows, :] * gain).astype(jnp.bfloat16)
+        out_ref[0, 1] = (up_ref[0, rows, :] * gain).astype(jnp.bfloat16)
+
+
+def cast(gate_weight, up_weight, gain_col, where, expert, halves):
+    _, rows, cols = gate_weight.shape
+    wide = cols // 2
+    weight_spec = pl.BlockSpec((1, rows, wide), lambda i: (expert, 0, i))
+    gain_spec = pl.BlockSpec((rows, 1), lambda i: (0, 0))
+    if not halves:
+        return pl.pallas_call(
+            cast_whole,
+            grid=(2,),
+            in_specs=[weight_spec, weight_spec, gain_spec],
+            out_specs=pl.BlockSpec((1, 2, rows, wide), lambda i: (i, 0, 0, 0)),
+            out_shape=jax.ShapeDtypeStruct((2, 2, rows, wide), jnp.bfloat16),
+        )(gate_weight, up_weight, gain_col)
+    out_spec = pl.BlockSpec((1, 2, rows // 2, wide), lambda i: (i, 0, 0, 0))
+    out = jax.ShapeDtypeStruct((2, 2, rows // 2, wide), jnp.bfloat16)
+    return pl.pallas_call(
+        cast_halves,
+        grid=(2,),
+        in_specs=[SMEM, weight_spec, weight_spec, gain_spec],
+        out_specs=[out_spec, out_spec],
+        out_shape=[out, out],
+    )(where, gate_weight, up_weight, gain_col)
+
+
+def pick_kernel(where_ref, own_ref, got_ref, *outs):
+    flag, y = where_ref[1], where_ref[2]
+    for r in range(2):
+        at = y if r == 0 else 1 - y
+
+        @pl.when(flag == 0)
+        def _():
+            outs[r][...] = own_ref[at]
+            outs[2 + r][...] = got_ref[at]
+
+        @pl.when(flag != 0)
+        def _():
+            outs[r][...] = got_ref[at]
+            outs[2 + r][...] = own_ref[at]
+
+
+def pick(where, own, got):
+    sides, kinds, rows, wide = own.shape
+    block = min(128, rows)
+    in_spec = pl.BlockSpec((sides, 1, block, wide), lambda i, j: (0, i, j, 0))
+    out_spec = pl.BlockSpec((1, block, wide), lambda i, j: (i, j, 0))
+    out = jax.ShapeDtypeStruct(own.shape[1:], own.dtype)
+    return pl.pallas_call(
+        pick_kernel,
+        grid=(kinds, rows // block),
+        in_specs=[SMEM, in_spec, in_spec],
+        out_specs=[out_spec] * 4,
+        out_shape=[out] * 4,
+    )(where, own, got)
+
+
+def expert_kernel(
+    where_ref, share_ref, normed_ref, *refs, expert, sizes, has_outs, has_acc, last, parts
+):
+    rows_in, pieces_n, downs_n = sizes
+    pieces, refs = refs[:pieces_n], refs[pieces_n:]
+    downs, refs = refs[:downs_n], refs[downs_n:]
+    if has_outs:
+        refs = refs[3:]
+    if has_acc:
+        acc_in, refs = refs[0], refs[1:]
+    (gate_out, up_out, down_out), refs = refs[:3], refs[3:]
+    if last:
+        final_refs, refs = refs[:parts], refs[parts:]
+    else:
+        acc_out, refs = refs[0], refs[1:]
+    gate_v, up_v, down_v, hidden_v, acc_v, in_sem, down_sem, out_sem, acc_sem = refs
+    base, x, tp, fs = where_ref[3], where_ref[0], where_ref[4], where_ref[5]
+    copies = [[], []]
+    for i in range(pieces_n):
+        if pieces_n == parts:
+            at = (base ^ i) * rows_in
+        else:
+            at = (base ^ (i // 2)) * (2 * rows_in) + (x ^ (i % 2)) * rows_in
+        rows = pl.ds(pl.multiple_of(at, rows_in), rows_in)
+        for kind, to in ((0, gate_v), (1, up_v)):
+            copies[kind].append(
+                pltpu.make_async_copy(
+                    pieces[i].at[kind], to.at[rows, :], in_sem.at[kind, i]
+                )
+            )
+    for kind in range(2):
+        for item in copies[kind]:
+            item.start()
+    wide = downs[0].shape[1]
+    down_copies = []
+    for i in range(downs_n):
+        cols = pl.ds(pl.multiple_of((tp ^ i) * wide, wide), wide)
+        item = pltpu.make_async_copy(downs[i], down_v.at[:, cols], down_sem.at[i])
+        item.start()
+        down_copies.append(item)
+    if has_acc:
+        acc_copy = pltpu.make_async_copy(acc_in, acc_v, acc_sem.at[0])
+        acc_copy.start()
+    leaves = [
+        pltpu.make_async_copy(gate_v, gate_out.at[expert], out_sem.at[0]),
+        pltpu.make_async_copy(up_v, up_out.at[expert], out_sem.at[1]),
+        pltpu.make_async_copy(down_v, down_out.at[expert], out_sem.at[2]),
+    ]
+    for kind in range(2):
+        for item in copies[kind]:
+            item.wait()
+        leaves[kind].start()
+    tokens = normed_ref.shape[0]
+    units = gate_v.shape[1]
+    step = min(256, units)
+    for n in range(units // step):
+        cols = slice(n * step, (n + 1) * step)
+        gate_val = jnp.dot(normed_ref[...], gate_v[:, cols], preferred_element_type=jnp.float32)
+        up_val = jnp.dot(normed_ref[...], up_v[:, cols], preferred_element_type=jnp.float32)
+        hidden_v[:, cols] = (gate_val / (1.0 + jnp.exp(-gate_val)) * up_val).astype(jnp.bfloat16)
+    for item in down_copies:
+        item.wait()
+    leaves[2].start()
+    if has_acc:
+        acc_copy.wait()
+    width = down_v.shape[1]
+    step = min(512, width)
+    share = share_ref[...]
+    for n in range(width // step):
+        cols = slice(n * step, (n + 1) * step)
+        result = share * jnp.dot(
+            hidden_v[...], down_v[:, cols], preferred_element_type=jnp.float32
+        )
+        acc_v[:, cols] = acc_v[:, cols] + result if has_acc else result
+    if last:
+        block = tokens // parts
+        for i in range(parts):
+            rows = pl.ds(pl.multiple_of((fs ^ i) * block, block), block)
+            final_refs[i][...] = acc_v[rows, :].astype(final_refs[i].dtype)
+    else:
+        acc_copy = pltpu.make_async_copy(acc_v, acc_out, acc_sem.at[0])
+        acc_copy.start()
+        acc_copy.wait()
+    for item in leaves:
+        item.wait()
+
+
+def expert_step(where, share, normed, pieces, downs, outs, acc, expert, experts, last, parts):
+    tokens, width = normed.shape
+    rows_in, units = pieces[0].shape[1:]
+    fan = downs[0].shape[0]
+    sizes = (rows_in, len(pieces), len(downs))
+    operands = [where, share, normed, *pieces, *downs]
+    specs = [SMEM, VMEM, VMEM] + [ANY] * (len(pieces) + len(downs))
+    aliases = {}
+    if outs is not None:
+        for i in range(3):
+            aliases[len(operands) + i] = i
+        operands += list(outs)
+        specs += [ANY] * 3
+    if acc is not None:
+        operands.append(acc)
+        specs.append(ANY)
+    shapes = [
+        jax.ShapeDtypeStruct((experts, width, units), jnp.bfloat16),
+        jax.ShapeDtypeStruct((experts, width, units), jnp.bfloat16),
+        jax.ShapeDtypeStruct((experts, fan, width), jnp.bfloat16),
+    ]
+    out_specs = [ANY] * 3
+    if last:
+        block = tokens // parts
+        for i in range(parts):
+            shapes.append(
+                jax.ShapeDtypeStruct((block, width), jnp.float32 if i == 0 else jnp.bfloat16)
+            )
+        out_specs += [VMEM] * parts
+    else:
+        shapes.append(jax.ShapeDtypeStruct((tokens, width), jnp.float32))
+        out_specs.append(ANY)
+    body = functools.partial(
+        expert_kernel,
+        expert=expert,
+        sizes=sizes,
+        has_outs=outs is not None,
+        has_acc=acc is not None,
+        last=last,
+        parts=parts,
+    )
+    flops = 6 * tokens * width * units
+    return pl.pallas_call(
+        body,
+        in_specs=specs,
+        out_specs=out_specs,
+        out_shape=shapes,
+        input_output_aliases=aliases,
+        scratch_shapes=[
+            pltpu.VMEM((width, units), jnp.bfloat16),
+            pltpu.VMEM((width, units), jnp.bfloat16),
+            pltpu.VMEM((fan, width), jnp.bfloat16),
+            pltpu.VMEM((tokens, units), jnp.bfloat16),
+            pltpu.VMEM((tokens, width), jnp.float32),
+            pltpu.SemaphoreType.DMA((2, len(pieces))),
+            pltpu.SemaphoreType.DMA((len(downs),)),
+            pltpu.SemaphoreType.DMA((3,)),
+            pltpu.SemaphoreType.DMA((1,)),
+        ],
+        compiler_params=pltpu.CompilerParams(vmem_limit_bytes=56 * 1024 * 1024),
+        cost_estimate=pl.CostEstimate(
+            flops=flops, transcendentals=tokens * units, bytes_accessed=6 * width * units
+        ),
+    )(*operands)
+
+
+def make_fast(fs_size, tp_size):
+    def table(target):
+        pairs = []
+        for f in range(fs_size):
+            for t in range(tp_size):
+                to_f, to_t = target(f, t)
+                pairs.append((f * tp_size + t, to_f * tp_size + to_t))
+        return pairs
+
+    across_x = table(lambda f, t: (f, t ^ 2))
+    across_core = table(lambda f, t: (f, t ^ 1))
+    plane = [
+        table(
+            lambda f, t, a=a, r=r: (
+                ((f >> 2) ^ a) << 2 | (t & 1) << 1 | ((f & 1) ^ r),
+                (t & 2) | ((f >> 1) & 1),
+            )
+        )
+        for a in range(2)
+        for r in range(2)
+    ]
+    shift = [table(lambda f, t, s=s: (f ^ s, t)) for s in range(fs_size)]
+
+    def send(value, pairs):
+        return lax.ppermute(value, ("fs", "tp"), pairs)
+
+    def fast(tokens, norm_gain, gate_weight, up_weight, down_weight, routes, route_logit):
+        experts = gate_weight.shape[0]
+        fs = lax.axis_index("fs")
+        tp = lax.axis_index("tp")
+        z1, y, x, c = fs >> 2, fs & 1, tp >> 1, tp & 1
+        base = ((fs >> 2) << 2) | (c << 1) | y
+        where = jnp.stack([x, z1 ^ x, y, base, tp, fs]).astype(jnp.int32)
+        gain_col = norm_gain[:, None]
+
+        floats = tokens.astype(jnp.float32)
+        normed = (
+            floats * lax.rsqrt(jnp.mean(floats * floats, axis=1, keepdims=True) + EPS)
+        ).astype(jnp.bfloat16)
+        first_share = jax.nn.sigmoid(route_logit[:, 0] - route_logit[:, 1])
+        shares = jnp.stack([first_share, 1.0 - first_share], axis=1)
+
+        picked = []
+        for e in range(experts):
+            halves = e == 0
+            if halves:
+                own, leave = cast(gate_weight, up_weight, gain_col, where, e, True)
+            else:
+                own = leave = cast(gate_weight, up_weight, gain_col, where, e, False)
+            got = send(leave, across_x)
+            picked.append(pick(where, own, got))
+        outs = acc = None
+        for e in range(experts):
+            halves = e == 0
+            here = [send(m, plane[i]) for i, m in enumerate(picked[e])]
+            near = [[m] for m in here]
+            if halves:
+                for i, m in enumerate(here):
+                    near[i].append(send(m, across_x))
+            far = [[send(m, across_core) for m in item] for item in near]
+            pieces = []
+            for k in range(fs_size):
+                source = far if k & 2 else near
+                pieces += source[(k >> 2) * 2 + (k & 1)]
+            down = down_weight[e].astype(jnp.bfloat16)
+            down_x = send(down, across_x)
+            downs = [down, send(down, across_core), down_x, send(down_x, across_core)]
+            share = jnp.sum(jnp.where(routes == e, shares, 0.0), axis=1, keepdims=True)
+            last = e == experts - 1
+            result = expert_step(
+                where, share, normed, pieces, downs, outs, acc, e, experts, last, fs_size
+            )
+            outs, acc = result[:3], result[3]
+        mixed = acc
+        for s in range(1, fs_size):
+            mixed = mixed + send(result[3 + s], shift[s]).astype(jnp.float32)
+        return (*outs, mixed.astype(jnp.bfloat16))
+
+    return fast
 
 
 def shards(tokens, norm_gain, gate_weight, up_weight, down_weight, routes, route_logit):
@@ -67,8 +380,16 @@
 
 
 def solution(mesh):
+    fs_size, tp_size = mesh.shape["fs"], mesh.shape["tp"]
+    fast = (fs_size, tp_size) == (8, 4)
+
+    def program(*args):
+        if not fast:
+            return shards(*args)
+        return make_fast(fs_size, tp_size)(*args)
+
     return jax.shard_map(
-        shards,
+        program,
         mesh=mesh,
         in_specs=(
             P("tp", None),

time: 961 us -> 769 us (0.80)
  the two profiles are of different devices: /device:TPU:0 before, /device:TPU:10 now
where the time goes in v1:
time: 769 us; the launch traced here: 762 us
  waiting for transfers between devices  551 us (72%)
  Pallas kernels  113 us (15%)
  starting transfers between devices  79.7 us (10%)
  other arithmetic  9.24 us (1%)
  local copies, waits for them, and re-layouts  8.26 us (1%)
    ppermute x63, waiting for transfers between devices, send(): return lax.ppermute(value, ('fs', 'tp'), pairs)  551 us
    pallas_call x4, Pallas kernels, expert_step(): pl.pallas_call(body, in_specs=specs, out_specs=out_specs, out_shape=shape...  82.4 us
    ppermute x63, starting transfers between devices, send(): return lax.ppermute(value, ('fs', 'tp'), pairs)  79.7 us
    pallas_call x4, Pallas kernels, pick(): pl.pallas_call(pick_kernel, grid=(kinds, rows // block), in_specs=[SMEM,...  17.1 us
  transfers between devices with their start and end apart: 63, of which 26 were waited for; matrix products, arithmetic and copies ran while one was open for 1% of the time, Pallas kernels for 12%

profile of v1, /device:TPU:10, one launch (start us, length us, event | category | flops | bytes accessed | tf_op | source)
XLA Modules:
  0.0 762.1 jit_solution(8969978878155892478)
XLA Ops:
  0.6 1.5 copy.20.gain_ref
  2.8 3.3 shard_map.108
  6.7 3.9 convert.6
  10.9 1.6 collective-permute-start.54
  13.2 19.1 %collective-permute-done.36.got_ref = bf16[2,2,128,1024]{3,2,1,0:T(8,128)(2,1)S(1)} collective-permute-done((bf16[2,2,128,1024]{3,2,1,0:T(8,128)(2,1)}, bf16[2,2,128,1024]{3,2,1,0:T(8,128)(2,1)S(1)}, u32[]{:S(2)}, u32[]{:S(2)}) %collective-permute-start.36) | collective-permute-done | bytes 1048608 | tf_op jit(solution)/shard_map/ppermute | solution.py:265
  32.9 22.0 %collective-permute-done.54.refs_18_ = bf16[1024,512]{1,0:T(8,128)(2,1)} collective-permute-done((bf16[1024,512]{1,0:T(8,128)(2,1)S(1)}, bf16[1024,512]{1,0:T(8,128)(2,1)}, u32[]{:S(2)}, u32[]{:S(2)}) %collective-permute-start.54) | collective-permute-done | bytes 1048608 | tf_op jit(solution)/shard_map/ppermute | solution.py:265
  55.5 21.8 %collective-permute-done.34.refs_10_ = bf16[1024,512]{1,0:T(8,128)(2,1)S(1)} collective-permute-done((bf16[1024,512]{1,0:T(8,128)(2,1)S(1)}, bf16[1024,512]{1,0:T(8,128)(2,1)S(1)}, u32[]{:S(2)}, u32[]{:S(2)}) %collective-permute-start.34) | collective-permute-done | bytes 1048608 | tf_op jit(solution)/shard_map/ppermute | solution.py:265
  77.3 1.0 copy-done.4
  78.4 2.6 shard_map.109
  81.0 2.5 collective-permute-start.37
  83.5 16.4 %collective-permute-done.22.refs_10_ = bf16[1024,512]{1,0:T(8,128)(2,1)} collective-permute-done((bf16[1024,512]{1,0:T(8,128)(2,1)S(1)}, bf16[1024,512]{1,0:T(8,128)(2,1)}, u32[]{:S(2)}, u32[]{:S(2)}) %collective-permute-start.22) | collective-permute-done | bytes 1048608 | tf_op jit(solution)/shard_map/ppermute | solution.py:265
  99.9 3.8 collective-permute-start.45
  103.7 17.5 %collective-permute-done.10.refs_10_ = bf16[1024,512]{1,0:T(8,128)(2,1)} collective-permute-done((bf16[1024,512]{1,0:T(8,128)(2,1)S(1)}, bf16[1024,512]{1,0:T(8,128)(2,1)}, u32[]{:S(2)}, u32[]{:S(2)}) %collective-permute-start.10) | collective-permute-done | bytes 1048608 | tf_op jit(solution)/shard_map/ppermute | solution.py:265
  121.2 1.1 collective-permute-start.47
  122.9 1.5 collective-permute-start.40
  124.4 12.6 %collective-permute-done.45.refs_8_ = bf16[2,128,1024]{2,1,0:T(8,128)(2,1)} collective-permute-done((bf16[2,128,1024]{2,1,0:T(8,128)(2,1)}, bf16[2,128,1024]{2,1,0:T(8,128)(2,1)}, u32[]{:S(2)}, u32[]{:S(2)}) %collective-permute-start.45) | collective-permute-done | bytes 524320 | tf_op jit(solution)/shard_map/ppermute | solution.py:265
  137.5 10.2 %collective-permute-done.47.refs_10_ = bf16[2,128,1024]{2,1,0:T(8,128)(2,1)} collective-permute-done((bf16[2,128,1024]{2,1,0:T(8,128)(2,1)}, bf16[2,128,1024]{2,1,0:T(8,128)(2,1)}, u32[]{:S(2)}, u32[]{:S(2)}) %collective-permute-start.47) | collective-permute-done | bytes 524320 | tf_op jit(solution)/shard_map/ppermute | solution.py:265
  148.2 3.4 shard_map.106.own_ref
  152.2 1.5 collective-permute-start.24
  153.7 6.1 collective-permute-done.46.refs_9_
  160.2 3.4 shard_map.104.own_ref
  163.6 7.4 collective-permute-done.48.refs_11_
  171.7 3.4 shard_map.102.own_ref
  175.1 1.6 collective-permute-start
  176.8 2.2 collective-permute-done.51.refs_14_
  179.5 36.5 %collective-permute-done.24.got_ref = bf16[2,2,256,1024]{3,2,1,0:T(8,128)(2,1)} collective-permute-done((bf16[2,2,256,1024]{3,2,1,0:T(8,128)(2,1)}, bf16[2,2,256,1024]{3,2,1,0:T(8,128)(2,1)}, u32[]{:S(2)}, u32[]{:S(2)}) %collective-permute-start.24) | collective-permute-done | bytes 2097184 | tf_op jit(solution)/shard_map/ppermute | solution.py:265
  216.5 44.4 %collective-permute-done.12.got_ref = bf16[2,2,256,1024]{3,2,1,0:T(8,128)(2,1)} collective-permute-done((bf16[2,2,256,1024]{3,2,1,0:T(8,128)(2,1)}, bf16[2,2,256,1024]{3,2,1,0:T(8,128)(2,1)}, u32[]{:S(2)}, u32[]{:S(2)}) %collective-permute-start.12) | collective-permute-done | bytes 2097184 | tf_op jit(solution)/shard_map/ppermute | solution.py:265
  261.4 4.9 shard_map.107
  266.3 4.8 shard_map.105
  271.1 34.7 %collective-permute-done.got_ref = bf16[2,2,256,1024]{3,2,1,0:T(8,128)(2,1)} collective-permute-done((bf16[2,2,256,1024]{3,2,1,0:T(8,128)(2,1)}, bf16[2,2,256,1024]{3,2,1,0:T(8,128)(2,1)}, u32[]{:S(2)}, u32[]{:S(2)}) %collective-permute-start) | collective-permute-done | bytes 2097184 | tf_op jit(solution)/shard_map/ppermute | solution.py:265
  305.8 4.5 collective-permute-start.25
  310.5 2.5 collective-permute-start.30
  313.1 5.6 collective-permute-start.13
  318.6 4.8 shard_map.103
  323.4 2.2 collective-permute-done.25.refs_0_
  325.6 22.2 %collective-permute-done.26.refs_1_ = bf16[2,256,1024]{2,1,0:T(8,128)(2,1)} collective-permute-done((bf16[2,256,1024]{2,1,0:T(8,128)(2,1)}, bf16[2,256,1024]{2,1,0:T(8,128)(2,1)}, u32[]{:S(2)}, u32[]{:S(2)}) %collective-permute-start.26) | collective-permute-done | bytes 1048608 | tf_op jit(solution)/shard_map/ppermute | solution.py:265
  347.8 3.8 collective-permute-start.18
  351.7 100.7 %collective-permute-done.30.refs_5_ = bf16[2,256,1024]{2,1,0:T(8,128)(2,1)} collective-permute-done((bf16[2,256,1024]{2,1,0:T(8,128)(2,1)}, bf16[2,256,1024]{2,1,0:T(8,128)(2,1)}, u32[]{:S(2)}, u32[]{:S(2)}) %collective-permute-start.30) | collective-permute-done | bytes 1048608 | tf_op jit(solution)/shard_map/ppermute | solution.py:265
  452.4 2.4 collective-permute-start.1
  454.8 2.5 collective-permute-start.2
  457.4 24.6 %collective-permute-done.17.refs_4_ = bf16[2,256,1024]{2,1,0:T(8,128)(2,1)} collective-permute-done((bf16[2,256,1024]{2,1,0:T(8,128)(2,1)}, bf16[2,256,1024]{2,1,0:T(8,128)(2,1)}, u32[]{:S(2)}, u32[]{:S(2)}) %collective-permute-start.17) | collective-permute-done | bytes 1048608 | tf_op jit(solution)/shard_map/ppermute | solution.py:265
  482.0 60.3 %collective-permute-done.18.refs_5_ = bf16[2,256,1024]{2,1,0:T(8,128)(2,1)} collective-permute-done((bf16[2,256,1024]{2,1,0:T(8,128)(2,1)}, bf16[2,256,1024]{2,1,0:T(8,128)(2,1)}, u32[]{:S(2)}, u32[]{:S(2)}) %collective-permute-start.18) | collective-permute-done | bytes 1048608 | tf_op jit(solution)/shard_map/ppermute | solution.py:265
  542.3 7.1 collective-permute-start.27
  550.6 2.2 fusion.1.normed_ref
  552.8 11.6 %collective-permute-done.5.refs_4_ = bf16[2,256,1024]{2,1,0:T(8,128)(2,1)S(1)} collective-permute-done((bf16[2,256,1024]{2,1,0:T(8,128)(2,1)}, bf16[2,256,1024]{2,1,0:T(8,128)(2,1)S(1)}, u32[]{:S(2)}, u32[]{:S(2)}) %collective-permute-start.5) | collective-permute-done | bytes 1048608 | tf_op jit(solution)/shard_map/ppermute | solution.py:265
  564.5 7.4 collective-permute-start.32
  571.9 15.2 %collective-permute-done.6.refs_5_ = bf16[2,256,1024]{2,1,0:T(8,128)(2,1)S(1)} collective-permute-done((bf16[2,256,1024]{2,1,0:T(8,128)(2,1)}, bf16[2,256,1024]{2,1,0:T(8,128)(2,1)S(1)}, u32[]{:S(2)}, u32[]{:S(2)}) %collective-permute-start.6) | collective-permute-done | bytes 1048608 | tf_op jit(solution)/shard_map/ppermute | solution.py:265
  587.1 2.8 collective-permute-start.15
  589.9 1.0 collective-permute-start.16
  595.1 20.7 %shard_map.110 = (bf16[4,2048,1024]{2,1,0:T(8,128)(2,1)}, bf16[4,2048,1024]{2,1,0:T(8,128)(2,1)}, bf16[4,1024,2048]{2,1,0:T(8,128)(2,1)}, f32[768,2048]{1,0:T(8,128)}) custom-call(s32[6]{0:T(128)} %stack.32.where_ref, f32[768,1]{1,0:T(8,128)} %broadcast_in_dim.32.share_ref, bf16[768,2048]{1,0:T(8,128)(2,1)} %fusion.1.normed_ref, ...), custom_call_target="tpu_custom_call" | custom-call | flops 9663676416 | bytes 12582912 | tf_op jit(solution)/shard_map/pallas_call | solution.py:217
  617.3 20.8 %shard_map.111 = (bf16[4,2048,1024]{2,1,0:T(8,128)(2,1)}, bf16[4,2048,1024]{2,1,0:T(8,128)(2,1)}, bf16[4,1024,2048]{2,1,0:T(8,128)(2,1)}, f32[768,2048]{1,0:T(8,128)}) custom-call(s32[6]{0:T(128)} %stack.32.where_ref, f32[768,1]{1,0:T(8,128)} %broadcast_in_dim.31.share_ref, ...), custom_call_target="tpu_custom_call", output_to_operand_aliasing={{0}: (15, {}), {1}: (16, {}), {2}: (17, {})} | custom-call | flops 9663676416 | bytes 12582912 | tf_op jit(solution)/shard_map/pallas_call | solution.py:217
  638.1 20.7 %shard_map.112 = (bf16[4,2048,1024]{2,1,0:T(8,128)(2,1)}, bf16[4,2048,1024]{2,1,0:T(8,128)(2,1)}, bf16[4,1024,2048]{2,1,0:T(8,128)(2,1)}, f32[768,2048]{1,0:T(8,128)}) custom-call(s32[6]{0:T(128)} %stack.32.where_ref, f32[768,1]{1,0:T(8,128)} %broadcast_in_dim.30.share_ref, ...), custom_call_target="tpu_custom_call", output_to_operand_aliasing={{0}: (15, {}), {1}: (16, {}), {2}: (17, {})} | custom-call | flops 9663676416 | bytes 12582912 | tf_op jit(solution)/shard_map/pallas_call | solution.py:217
  658.9 1.0 copy-done.16
  659.9 20.3 %shard_map.113 = (bf16[4,2048,1024]{2,1,0:T(8,128)(2,1)}, bf16[4,2048,1024]{2,1,0:T(8,128)(2,1)}, bf16[4,1024,2048]{2,1,0:T(8,128)(2,1)}, f32[96,2048]{1,0:T(8,1...) custom-call(s32[6]{0:T(128)} %stack.32.where_ref, ...), custom_call_target="tpu_custom_call", output_to_operand_aliasing={{0}: (15, {}), {1}: (16, {}), {2}: (17, {})} | custom-call | flops 9663676416 | bytes 12582912 | tf_op jit(solution)/shard_map/pallas_call | solution.py:217
  680.9 6.5 collective-permute-start.57
  687.7 3.5 collective-permute-start.60
  691.7 3.9 collective-permute-start.61
  695.7 14.3 %collective-permute-done.57 = bf16[96,2048]{1,0:T(8,128)(2,1)S(1)} collective-permute-done((bf16[96,2048]{1,0:T(8,128)(2,1)}, bf16[96,2048]{1,0:T(8,128)(2,1)S(1)}, u32[]{:S(2)}, u32[]{:S(2)}) %collective-permute-start.57) | collective-permute-done | bytes 393248 | tf_op jit(solution)/shard_map/ppermute | solution.py:265
  710.0 1.4 collective-permute-start.62
  711.4 6.0 collective-permute-done.58
  717.4 22.3 %collective-permute-done.60 = bf16[96,2048]{1,0:T(8,128)(2,1)S(1)} collective-permute-done((bf16[96,2048]{1,0:T(8,128)(2,1)}, bf16[96,2048]{1,0:T(8,128)(2,1)S(1)}, u32[]{:S(2)}, u32[]{:S(2)}) %collective-permute-start.60) | collective-permute-done | bytes 393248 | tf_op jit(solution)/shard_map/ppermute | solution.py:265
  739.7 12.2 %collective-permute-done.61 = bf16[96,2048]{1,0:T(8,128)(2,1)S(1)} collective-permute-done((bf16[96,2048]{1,0:T(8,128)(2,1)}, bf16[96,2048]{1,0:T(8,128)(2,1)S(1)}, u32[]{:S(2)}, u32[]{:S(2)}) %collective-permute-start.61) | collective-permute-done | bytes 393248 | tf_op jit(solution)/shard_map/ppermute | solution.py:265
  752.0 7.5 collective-permute-done.62
  759.5 2.4 add_convert_fusion
  (132 shorter events, 17.2 us)
Async XLA Ops:
  6.1 26.2 %collective-permute-start.36 = (bf16[2,2,128,1024]{3,2,1,0:T(8,128)(2,1)}, bf16[2,2,128,1024]{3,2,1,0:T(8,128)(2,1)S(1)}, u32[]{:S(2)}, u32[]{:S(2)}) collective-permute-start(bf16[2,2,128,1024]{3,2,1,0:T(8,128)(2,1)} %get-tuple-element.58), channel_id=1, source_target_pairs={{0,2},{1,3},{2,0},{3,1},{4,6},{5,7},{6,4},{7,5},{8,10},{9,11},{10,... | collective-permute-start | bytes 3145736 | tf_op jit(solution)/shard_map/ppermute | solution.py:265
  10.9 44.0 %collective-permute-start.54 = (bf16[1024,512]{1,0:T(8,128)(2,1)S(1)}, bf16[1024,512]{1,0:T(8,128)(2,1)}, u32[]{:S(2)}, u32[]{:S(2)}) collective-permute-start(bf16[1024,512]{1,0:T(8,128)(2,1)S(1)} %get-tuple-element.92.refs_16_), channel_id=1, source_target_pairs={{0,2},{1,3},{2,0},{3,1},{4,6},{5,7},{6,4},{7,5},{8,10},{9,11},{10,... | collective-permute-start | bytes 3145736 | tf_op jit(solution)/shard_map/ppermute | solution.py:265
  12.5 42.5 %collective-permute-start.53 = (bf16[1024,512]{1,0:T(8,128)(2,1)S(1)}, bf16[1024,512]{1,0:T(8,128)(2,1)S(1)}, u32[]{:S(2)}, u32[]{:S(2)}) collective-permute-start(bf16[1024,512]{1,0:T(8,128)(2,1)S(1)} %get-tuple-element.92.refs_16_), channel_id=1, source_target_pairs={{0,1},{1,0},{2,3},{3,2},{4,5},{5,4},{6,7},{7,6},{8,9},{9,8},{10,11... | collective-permute-start | bytes 3145736 | tf_op jit(solution)/shard_map/ppermute | solution.py:265
  12.5 64.8 %collective-permute-start.34 = (bf16[1024,512]{1,0:T(8,128)(2,1)S(1)}, bf16[1024,512]{1,0:T(8,128)(2,1)S(1)}, u32[]{:S(2)}, u32[]{:S(2)}) collective-permute-start(bf16[1024,512]{1,0:T(8,128)(2,1)S(1)} %get-tuple-element.93.refs_8_), channel_id=1, source_target_pairs={{0,2},{1,3},{2,0},{3,1},{4,6},{5,7},{6,4},{7,5},{8,10},{9,11},{10,... | collective-permute-start | bytes 3145736 | tf_op jit(solution)/shard_map/ppermute | solution.py:265
  13.0 68.0 %collective-permute-start.33 = (bf16[1024,512]{1,0:T(8,128)(2,1)S(1)}, bf16[1024,512]{1,0:T(8,128)(2,1)}, u32[]{:S(2)}, u32[]{:S(2)}) collective-permute-start(bf16[1024,512]{1,0:T(8,128)(2,1)S(1)} %get-tuple-element.93.refs_8_), channel_id=1, source_target_pairs={{0,1},{1,0},{2,3},{3,2},{4,5},{5,4},{6,7},{7,6},{8,9},{9,8},{10,11... | collective-permute-start | bytes 3145736 | tf_op jit(solution)/shard_map/ppermute | solution.py:265
  32.4 67.5 %collective-permute-start.22 = (bf16[1024,512]{1,0:T(8,128)(2,1)S(1)}, bf16[1024,512]{1,0:T(8,128)(2,1)}, u32[]{:S(2)}, u32[]{:S(2)}) collective-permute-start(bf16[1024,512]{1,0:T(8,128)(2,1)S(1)} %get-tuple-element.94.refs_8_), channel_id=1, source_target_pairs={{0,2},{1,3},{2,0},{3,1},{4,6},{5,7},{6,4},{7,5},{8,10},{9,11},{10,... | collective-permute-start | bytes 3145736 | tf_op jit(solution)/shard_map/ppermute | solution.py:265
  54.9 44.9 %collective-permute-start.21 = (bf16[1024,512]{1,0:T(8,128)(2,1)S(1)}, bf16[1024,512]{1,0:T(8,128)(2,1)}, u32[]{:S(2)}, u32[]{:S(2)}) collective-permute-start(bf16[1024,512]{1,0:T(8,128)(2,1)S(1)} %get-tuple-element.94.refs_8_), channel_id=1, source_target_pairs={{0,1},{1,0},{2,3},{3,2},{4,5},{5,4},{6,7},{7,6},{8,9},{9,8},{10,11... | collective-permute-start | bytes 3145736 | tf_op jit(solution)/shard_map/ppermute | solution.py:265
  54.9 66.3 %collective-permute-start.10 = (bf16[1024,512]{1,0:T(8,128)(2,1)S(1)}, bf16[1024,512]{1,0:T(8,128)(2,1)}, u32[]{:S(2)}, u32[]{:S(2)}) collective-permute-start(bf16[1024,512]{1,0:T(8,128)(2,1)S(1)} %get-tuple-element.95.refs_8_), channel_id=1, source_target_pairs={{0,2},{1,3},{2,0},{3,1},{4,6},{5,7},{6,4},{7,5},{8,10},{9,11},{10,... | collective-permute-start | bytes 3145736 | tf_op jit(solution)/shard_map/ppermute | solution.py:265
  78.4 69.8 %collective-permute-start.9 = (bf16[1024,512]{1,0:T(8,128)(2,1)S(1)}, bf16[1024,512]{1,0:T(8,128)(2,1)}, u32[]{:S(2)}, u32[]{:S(2)}) collective-permute-start(bf16[1024,512]{1,0:T(8,128)(2,1)S(1)} %get-tuple-element.95.refs_8_), channel_id=1, source_target_pairs={{0,1},{1,0},{2,3},{3,2},{4,5},{5,4},{6,7},{7,6},{8,9},{9,8},{10,11... | collective-permute-start | bytes 3145736 | tf_op jit(solution)/shard_map/ppermute | solution.py:265
  81.0 41.3 %collective-permute-start.37 = (bf16[2,128,1024]{2,1,0:T(8,128)(2,1)}, bf16[2,128,1024]{2,1,0:T(8,128)(2,1)}, u32[]{:S(2)}, u32[]{:S(2)}) collective-permute-start(bf16[2,128,1024]{2,1,0:T(8,128)(2,1)} %get-tuple-element.59), channel_id=1, source_target_pairs={{0,0},{1,8},{2,2},{3,10},{4,4},{5,12},{6,6},{7,14},{8,1},{9,9},{10... | collective-permute-start | bytes 1572872 | tf_op jit(solution)/shard_map/ppermute | solution.py:265
  99.9 23.0 %collective-permute-start.39 = (bf16[2,128,1024]{2,1,0:T(8,128)(2,1)}, bf16[2,128,1024]{2,1,0:T(8,128)(2,1)}, u32[]{:S(2)}, u32[]{:S(2)}) collective-permute-start(bf16[2,128,1024]{2,1,0:T(8,128)(2,1)} %get-tuple-element.60), channel_id=1, source_target_pairs={{0,4},{1,12},{2,6},{3,14},{4,0},{5,8},{6,2},{7,10},{8,5},{9,13},{1... | collective-permute-start | bytes 1572872 | tf_op jit(solution)/shard_map/ppermute | solution.py:265
  99.9 37.1 %collective-permute-start.45 = (bf16[2,128,1024]{2,1,0:T(8,128)(2,1)}, bf16[2,128,1024]{2,1,0:T(8,128)(2,1)}, u32[]{:S(2)}, u32[]{:S(2)}) collective-permute-start(bf16[2,128,1024]{2,1,0:T(8,128)(2,1)} %get-tuple-element.61), channel_id=1, source_target_pairs={{0,16},{1,24},{2,18},{3,26},{4,20},{5,28},{6,22},{7,30},{8,17},{9,... | collective-permute-start | bytes 1572872 | tf_op jit(solution)/shard_map/ppermute | solution.py:265
  121.2 26.4 %collective-permute-start.47 = (bf16[2,128,1024]{2,1,0:T(8,128)(2,1)}, bf16[2,128,1024]{2,1,0:T(8,128)(2,1)}, u32[]{:S(2)}, u32[]{:S(2)}) collective-permute-start(bf16[2,128,1024]{2,1,0:T(8,128)(2,1)} %get-tuple-element.62), channel_id=1, source_target_pairs={{0,20},{1,28},{2,22},{3,30},{4,16},{5,24},{6,18},{7,26},{8,21},{9,... | collective-permute-start | bytes 1572872 | tf_op jit(solution)/shard_map/ppermute | solution.py:265
  122.3 29.3 %collective-permute-start.38 = (bf16[2,128,1024]{2,1,0:T(8,128)(2,1)}, bf16[2,128,1024]{2,1,0:T(8,128)(2,1)}, u32[]{:S(2)}, u32[]{:S(2)}) collective-permute-start(bf16[2,128,1024]{2,1,0:T(8,128)(2,1)} %collective-permute-done.37.refs_0_), channel_id=1, source_target_pairs={{0,2},{1,3},{2,0},{3,1},{4,6},{5,7},{6,4},{7,5},{8,10},{9,11},{10,... | collective-permute-start | bytes 1572872 | tf_op jit(solution)/shard_map/ppermute | solution.py:265
  122.9 29.3 %collective-permute-start.40 = (bf16[2,128,1024]{2,1,0:T(8,128)(2,1)}, bf16[2,128,1024]{2,1,0:T(8,128)(2,1)}, u32[]{:S(2)}, u32[]{:S(2)}) collective-permute-start(bf16[2,128,1024]{2,1,0:T(8,128)(2,1)} %collective-permute-done.39.refs_2_), channel_id=1, source_target_pairs={{0,2},{1,3},{2,0},{3,1},{4,6},{5,7},{6,4},{7,5},{8,10},{9,11},{10,... | collective-permute-start | bytes 1572872 | tf_op jit(solution)/shard_map/ppermute | solution.py:265
  137.0 22.8 %collective-permute-start.46 = (bf16[2,128,1024]{2,1,0:T(8,128)(2,1)}, bf16[2,128,1024]{2,1,0:T(8,128)(2,1)}, u32[]{:S(2)}, u32[]{:S(2)}) collective-permute-start(bf16[2,128,1024]{2,1,0:T(8,128)(2,1)} %collective-permute-done.45.refs_8_), channel_id=1, source_target_pairs={{0,2},{1,3},{2,0},{3,1},{4,6},{5,7},{6,4},{7,5},{8,10},{9,11},{10,... | collective-permute-start | bytes 1572872 | tf_op jit(solution)/shard_map/ppermute | solution.py:265
  147.7 23.3 %collective-permute-start.48 = (bf16[2,128,1024]{2,1,0:T(8,128)(2,1)}, bf16[2,128,1024]{2,1,0:T(8,128)(2,1)}, u32[]{:S(2)}, u32[]{:S(2)}) collective-permute-start(bf16[2,128,1024]{2,1,0:T(8,128)(2,1)} %collective-permute-done.47.refs_10_), channel_id=1, source_target_pairs={{0,2},{1,3},{2,0},{3,1},{4,6},{5,7},{6,4},{7,5},{8,10},{9,11},{10,... | collective-permute-start | bytes 1572872 | tf_op jit(solution)/shard_map/ppermute | solution.py:265
  148.2 23.3 %collective-permute-start.41 = (bf16[2,128,1024]{2,1,0:T(8,128)(2,1)}, bf16[2,128,1024]{2,1,0:T(8,128)(2,1)}, u32[]{:S(2)}, u32[]{:S(2)}) collective-permute-start(bf16[2,128,1024]{2,1,0:T(8,128)(2,1)} %collective-permute-done.37.refs_0_), channel_id=1, source_target_pairs={{0,1},{1,0},{2,3},{3,2},{4,5},{5,4},{6,7},{7,6},{8,9},{9,8},{10,11... | collective-permute-start | bytes 1572872 | tf_op jit(solution)/shard_map/ppermute | solution.py:265
  151.6 23.5 %collective-permute-start.43 = (bf16[2,128,1024]{2,1,0:T(8,128)(2,1)}, bf16[2,128,1024]{2,1,0:T(8,128)(2,1)}, u32[]{:S(2)}, u32[]{:S(2)}) collective-permute-start(bf16[2,128,1024]{2,1,0:T(8,128)(2,1)} %collective-permute-done.39.refs_2_), channel_id=1, source_target_pairs={{0,1},{1,0},{2,3},{3,2},{4,5},{5,4},{6,7},{7,6},{8,9},{9,8},{10,11... | collective-permute-start | bytes 1572872 | tf_op jit(solution)/shard_map/ppermute | solution.py:265
  152.2 63.8 %collective-permute-start.24 = (bf16[2,2,256,1024]{3,2,1,0:T(8,128)(2,1)}, bf16[2,2,256,1024]{3,2,1,0:T(8,128)(2,1)}, u32[]{:S(2)}, u32[]{:S(2)}) collective-permute-start(bf16[2,2,256,1024]{3,2,1,0:T(8,128)(2,1)} %shard_map.106.own_ref), channel_id=1, source_target_pairs={{0,2},{1,3},{2,0},{3,1},{4,6},{5,7},{6,4},{7,5},{8,10},{9,11},{10,... | collective-permute-start | bytes 6291464 | tf_op jit(solution)/shard_map/ppermute | solution.py:265
  159.8 16.9 %collective-permute-start.49 = (bf16[2,128,1024]{2,1,0:T(8,128)(2,1)}, bf16[2,128,1024]{2,1,0:T(8,128)(2,1)}, u32[]{:S(2)}, u32[]{:S(2)}) collective-permute-start(bf16[2,128,1024]{2,1,0:T(8,128)(2,1)} %collective-permute-done.45.refs_8_), channel_id=1, source_target_pairs={{0,1},{1,0},{2,3},{3,2},{4,5},{5,4},{6,7},{7,6},{8,9},{9,8},{10,11... | collective-permute-start | bytes 1572872 | tf_op jit(solution)/shard_map/ppermute | solution.py:265
  171.0 89.9 %collective-permute-start.12 = (bf16[2,2,256,1024]{3,2,1,0:T(8,128)(2,1)}, bf16[2,2,256,1024]{3,2,1,0:T(8,128)(2,1)}, u32[]{:S(2)}, u32[]{:S(2)}) collective-permute-start(bf16[2,2,256,1024]{3,2,1,0:T(8,128)(2,1)} %shard_map.104.own_ref), channel_id=1, source_target_pairs={{0,2},{1,3},{2,0},{3,1},{4,6},{5,7},{6,4},{7,5},{8,10},{9,11},{10,... | collective-permute-start | bytes 6291464 | tf_op jit(solution)/shard_map/ppermute | solution.py:265
  171.5 7.5 collective-permute-start.55
  175.1 374.8 %copy-start = (bf16[768,2048]{1,0:T(8,128)(2,1)S(1)}, bf16[768,2048]{1,0:T(8,128)(2,1)}, u32[]{:S(2)}) copy-start(bf16[768,2048]{1,0:T(8,128)(2,1)} %param.7) | copy-start | bytes 9437188
  175.1 130.7 %collective-permute-start = (bf16[2,2,256,1024]{3,2,1,0:T(8,128)(2,1)}, bf16[2,2,256,1024]{3,2,1,0:T(8,128)(2,1)}, u32[]{:S(2)}, u32[]{:S(2)}) collective-permute-start(bf16[2,2,256,1024]{3,2,1,0:T(8,128)(2,1)} %shard_map.102.own_ref), channel_id=1, source_target_pairs={{0,2},{1,3},{2,0},{3,1},{4,6},{5,7},{6,4},{7,5},{8,10},{9,11},{10,... | collective-permute-start | bytes 6291464 | tf_op jit(solution)/shard_map/ppermute | solution.py:265
  176.7 2.3 collective-permute-start.51
  178.9 37.4 %collective-permute-start.35 = (bf16[1024,512]{1,0:T(8,128)(2,1)}, bf16[1024,512]{1,0:T(8,128)(2,1)}, u32[]{:S(2)}, u32[]{:S(2)}) collective-permute-start(bf16[1024,512]{1,0:T(8,128)(2,1)} %copy-done.4), channel_id=1, source_target_pairs={{0,1},{1,0},{2,3},{3,2},{4,5},{5,4},{6,7},{7,6},{8,9},{9,8},{10,11... | collective-permute-start | bytes 3145736 | tf_op jit(solution)/shard_map/ppermute | solution.py:265
  179.1 82.2 %collective-permute-start.23 = (bf16[1024,512]{1,0:T(8,128)(2,1)}, bf16[1024,512]{1,0:T(8,128)(2,1)}, u32[]{:S(2)}, u32[]{:S(2)}) collective-permute-start(bf16[1024,512]{1,0:T(8,128)(2,1)} %collective-permute-done.22.refs_10_), channel_id=1, source_target_pairs={{0,1},{1,0},{2,3},{3,2},{4,5},{5,4},{6,7},{7,6},{8,9},{9,8},{10,11... | collective-permute-start | bytes 3145736 | tf_op jit(solution)/shard_map/ppermute | solution.py:265
  215.9 94.4 %collective-permute-start.42 = (bf16[2,128,1024]{2,1,0:T(8,128)(2,1)}, bf16[2,128,1024]{2,1,0:T(8,128)(2,1)}, u32[]{:S(2)}, u32[]{:S(2)}) collective-permute-start(bf16[2,128,1024]{2,1,0:T(8,128)(2,1)} %collective-permute-done.38.refs_1_), channel_id=1, source_target_pairs={{0,1},{1,0},{2,3},{3,2},{4,5},{5,4},{6,7},{7,6},{8,9},{9,8},{10,11... | collective-permute-start | bytes 1572872 | tf_op jit(solution)/shard_map/ppermute | solution.py:265
  216.4 94.0 %collective-permute-start.44 = (bf16[2,128,1024]{2,1,0:T(8,128)(2,1)}, bf16[2,128,1024]{2,1,0:T(8,128)(2,1)}, u32[]{:S(2)}, u32[]{:S(2)}) collective-permute-start(bf16[2,128,1024]{2,1,0:T(8,128)(2,1)} %collective-permute-done.40.refs_3_), channel_id=1, source_target_pairs={{0,1},{1,0},{2,3},{3,2},{4,5},{5,4},{6,7},{7,6},{8,9},{9,8},{10,11... | collective-permute-start | bytes 1572872 | tf_op jit(solution)/shard_map/ppermute | solution.py:265
  260.9 49.6 %collective-permute-start.50 = (bf16[2,128,1024]{2,1,0:T(8,128)(2,1)}, bf16[2,128,1024]{2,1,0:T(8,128)(2,1)}, u32[]{:S(2)}, u32[]{:S(2)}) collective-permute-start(bf16[2,128,1024]{2,1,0:T(8,128)(2,1)} %collective-permute-done.46.refs_9_), channel_id=1, source_target_pairs={{0,1},{1,0},{2,3},{3,2},{4,5},{5,4},{6,7},{7,6},{8,9},{9,8},{10,11... | collective-permute-start | bytes 1572872 | tf_op jit(solution)/shard_map/ppermute | solution.py:265
  261.3 51.8 %collective-permute-start.52 = (bf16[2,128,1024]{2,1,0:T(8,128)(2,1)}, bf16[2,128,1024]{2,1,0:T(8,128)(2,1)}, u32[]{:S(2)}, u32[]{:S(2)}) collective-permute-start(bf16[2,128,1024]{2,1,0:T(8,128)(2,1)} %collective-permute-done.48.refs_11_), channel_id=1, source_target_pairs={{0,1},{1,0},{2,3},{3,2},{4,5},{5,4},{6,7},{7,6},{8,9},{9,8},{10,11... | collective-permute-start | bytes 1572872 | tf_op jit(solution)/shard_map/ppermute | solution.py:265
  305.8 19.8 %collective-permute-start.25 = (bf16[2,256,1024]{2,1,0:T(8,128)(2,1)}, bf16[2,256,1024]{2,1,0:T(8,128)(2,1)}, u32[]{:S(2)}, u32[]{:S(2)}) collective-permute-start(bf16[2,256,1024]{2,1,0:T(8,128)(2,1)} %get-tuple-element.53), channel_id=1, source_target_pairs={{0,0},{1,8},{2,2},{3,10},{4,4},{5,12},{6,6},{7,14},{8,1},{9,9},{10... | collective-permute-start | bytes 3145736 | tf_op jit(solution)/shard_map/ppermute | solution.py:265
  310.3 37.5 %collective-permute-start.26 = (bf16[2,256,1024]{2,1,0:T(8,128)(2,1)}, bf16[2,256,1024]{2,1,0:T(8,128)(2,1)}, u32[]{:S(2)}, u32[]{:S(2)}) collective-permute-start(bf16[2,256,1024]{2,1,0:T(8,128)(2,1)} %get-tuple-element.54), channel_id=1, source_target_pairs={{0,4},{1,12},{2,6},{3,14},{4,0},{5,8},{6,2},{7,10},{8,5},{9,13},{1... | collective-permute-start | bytes 3145736 | tf_op jit(solution)/shard_map/ppermute | solution.py:265
  310.4 37.4 %collective-permute-start.29 = (bf16[2,256,1024]{2,1,0:T(8,128)(2,1)}, bf16[2,256,1024]{2,1,0:T(8,128)(2,1)}, u32[]{:S(2)}, u32[]{:S(2)}) collective-permute-start(bf16[2,256,1024]{2,1,0:T(8,128)(2,1)} %get-tuple-element.55), channel_id=1, source_target_pairs={{0,16},{1,24},{2,18},{3,26},{4,20},{5,28},{6,22},{7,30},{8,17},{9,... | collective-permute-start | bytes 3145736 | tf_op jit(solution)/shard_map/ppermute | solution.py:265
  310.5 141.9 %collective-permute-start.30 = (bf16[2,256,1024]{2,1,0:T(8,128)(2,1)}, bf16[2,256,1024]{2,1,0:T(8,128)(2,1)}, u32[]{:S(2)}, u32[]{:S(2)}) collective-permute-start(bf16[2,256,1024]{2,1,0:T(8,128)(2,1)} %get-tuple-element.56), channel_id=1, source_target_pairs={{0,20},{1,28},{2,22},{3,30},{4,16},{5,24},{6,18},{7,26},{8,21},{9,... | collective-permute-start | bytes 3145736 | tf_op jit(solution)/shard_map/ppermute | solution.py:265
  313.1 141.7 %collective-permute-start.13 = (bf16[2,256,1024]{2,1,0:T(8,128)(2,1)}, bf16[2,256,1024]{2,1,0:T(8,128)(2,1)}, u32[]{:S(2)}, u32[]{:S(2)}) collective-permute-start(bf16[2,256,1024]{2,1,0:T(8,128)(2,1)} %get-tuple-element.49), channel_id=1, source_target_pairs={{0,0},{1,8},{2,2},{3,10},{4,4},{5,12},{6,6},{7,14},{8,1},{9,9},{10... | collective-permute-start | bytes 3145736 | tf_op jit(solution)/shard_map/ppermute | solution.py:265
  325.6 131.7 %collective-permute-start.14 = (bf16[2,256,1024]{2,1,0:T(8,128)(2,1)}, bf16[2,256,1024]{2,1,0:T(8,128)(2,1)S(1)}, u32[]{:S(2)}, u32[]{:S(2)}) collective-permute-start(bf16[2,256,1024]{2,1,0:T(8,128)(2,1)} %get-tuple-element.50), channel_id=1, source_target_pairs={{0,4},{1,12},{2,6},{3,14},{4,0},{5,8},{6,2},{7,10},{8,5},{9,13},{1... | collective-permute-start | bytes 3145736 | tf_op jit(solution)/shard_map/ppermute | solution.py:265
  347.8 134.1 %collective-permute-start.17 = (bf16[2,256,1024]{2,1,0:T(8,128)(2,1)}, bf16[2,256,1024]{2,1,0:T(8,128)(2,1)}, u32[]{:S(2)}, u32[]{:S(2)}) collective-permute-start(bf16[2,256,1024]{2,1,0:T(8,128)(2,1)} %get-tuple-element.51), channel_id=1, source_target_pairs={{0,16},{1,24},{2,18},{3,26},{4,20},{5,28},{6,22},{7,30},{8,17},{9,... | collective-permute-start | bytes 3145736 | tf_op jit(solution)/shard_map/ppermute | solution.py:265
  347.8 194.4 %collective-permute-start.18 = (bf16[2,256,1024]{2,1,0:T(8,128)(2,1)}, bf16[2,256,1024]{2,1,0:T(8,128)(2,1)}, u32[]{:S(2)}, u32[]{:S(2)}) collective-permute-start(bf16[2,256,1024]{2,1,0:T(8,128)(2,1)} %get-tuple-element.52), channel_id=1, source_target_pairs={{0,20},{1,28},{2,22},{3,30},{4,16},{5,24},{6,18},{7,26},{8,21},{9,... | collective-permute-start | bytes 3145736 | tf_op jit(solution)/shard_map/ppermute | solution.py:265
  452.4 97.0 %collective-permute-start.1 = (bf16[2,256,1024]{2,1,0:T(8,128)(2,1)}, bf16[2,256,1024]{2,1,0:T(8,128)(2,1)S(1)}, u32[]{:S(2)}, u32[]{:S(2)}) collective-permute-start(bf16[2,256,1024]{2,1,0:T(8,128)(2,1)} %get-tuple-element.45), channel_id=1, source_target_pairs={{0,0},{1,8},{2,2},{3,10},{4,4},{5,12},{6,6},{7,14},{8,1},{9,9},{10... | collective-permute-start | bytes 3145736 | tf_op jit(solution)/shard_map/ppermute | solution.py:265
  454.8 94.7 %collective-permute-start.2 = (bf16[2,256,1024]{2,1,0:T(8,128)(2,1)}, bf16[2,256,1024]{2,1,0:T(8,128)(2,1)S(1)}, u32[]{:S(2)}, u32[]{:S(2)}) collective-permute-start(bf16[2,256,1024]{2,1,0:T(8,128)(2,1)} %get-tuple-element.46), channel_id=1, source_target_pairs={{0,4},{1,12},{2,6},{3,14},{4,0},{5,8},{6,2},{7,10},{8,5},{9,13},{1... | collective-permute-start | bytes 3145736 | tf_op jit(solution)/shard_map/ppermute | solution.py:265
  457.3 107.2 %collective-permute-start.5 = (bf16[2,256,1024]{2,1,0:T(8,128)(2,1)}, bf16[2,256,1024]{2,1,0:T(8,128)(2,1)S(1)}, u32[]{:S(2)}, u32[]{:S(2)}) collective-permute-start(bf16[2,256,1024]{2,1,0:T(8,128)(2,1)} %get-tuple-element.47), channel_id=1, source_target_pairs={{0,16},{1,24},{2,18},{3,26},{4,20},{5,28},{6,22},{7,30},{8,17},{9,... | collective-permute-start | bytes 3145736 | tf_op jit(solution)/shard_map/ppermute | solution.py:265
  482.0 105.1 %collective-permute-start.6 = (bf16[2,256,1024]{2,1,0:T(8,128)(2,1)}, bf16[2,256,1024]{2,1,0:T(8,128)(2,1)S(1)}, u32[]{:S(2)}, u32[]{:S(2)}) collective-permute-start(bf16[2,256,1024]{2,1,0:T(8,128)(2,1)} %get-tuple-element.48), channel_id=1, source_target_pairs={{0,20},{1,28},{2,22},{3,30},{4,16},{5,24},{6,18},{7,26},{8,21},{9,... | collective-permute-start | bytes 3145736 | tf_op jit(solution)/shard_map/ppermute | solution.py:265
  542.3 47.6 %collective-permute-start.27 = (bf16[2,256,1024]{2,1,0:T(8,128)(2,1)}, bf16[2,256,1024]{2,1,0:T(8,128)(2,1)S(1)}, u32[]{:S(2)}, u32[]{:S(2)}) collective-permute-start(bf16[2,256,1024]{2,1,0:T(8,128)(2,1)} %collective-permute-done.25.refs_0_), channel_id=1, source_target_pairs={{0,1},{1,0},{2,3},{3,2},{4,5},{5,4},{6,7},{7,6},{8,9},{9,8},{10,11... | collective-permute-start | bytes 3145736 | tf_op jit(solution)/shard_map/ppermute | solution.py:265
  549.4 41.4 %collective-permute-start.28 = (bf16[2,256,1024]{2,1,0:T(8,128)(2,1)}, bf16[2,256,1024]{2,1,0:T(8,128)(2,1)S(1)}, u32[]{:S(2)}, u32[]{:S(2)}) collective-permute-start(bf16[2,256,1024]{2,1,0:T(8,128)(2,1)} %collective-permute-done.26.refs_1_), channel_id=1, source_target_pairs={{0,1},{1,0},{2,3},{3,2},{4,5},{5,4},{6,7},{7,6},{8,9},{9,8},{10,11... | collective-permute-start | bytes 3145736 | tf_op jit(solution)/shard_map/ppermute | solution.py:265
  549.5 41.4 %collective-permute-start.31 = (bf16[2,256,1024]{2,1,0:T(8,128)(2,1)}, bf16[2,256,1024]{2,1,0:T(8,128)(2,1)S(1)}, u32[]{:S(2)}, u32[]{:S(2)}) collective-permute-start(bf16[2,256,1024]{2,1,0:T(8,128)(2,1)} %collective-permute-done.29.refs_4_), channel_id=1, source_target_pairs={{0,1},{1,0},{2,3},{3,2},{4,5},{5,4},{6,7},{7,6},{8,9},{9,8},{10,11... | collective-permute-start | bytes 3145736 | tf_op jit(solution)/shard_map/ppermute | solution.py:265
  564.5 51.4 %collective-permute-start.32 = (bf16[2,256,1024]{2,1,0:T(8,128)(2,1)}, bf16[2,256,1024]{2,1,0:T(8,128)(2,1)}, u32[]{:S(2)}, u32[]{:S(2)}) collective-permute-start(bf16[2,256,1024]{2,1,0:T(8,128)(2,1)} %collective-permute-done.30.refs_5_), channel_id=1, source_target_pairs={{0,1},{1,0},{2,3},{3,2},{4,5},{5,4},{6,7},{7,6},{8,9},{9,8},{10,11... | collective-permute-start | bytes 3145736 | tf_op jit(solution)/shard_map/ppermute | solution.py:265
  587.1 29.1 %collective-permute-start.15 = (bf16[2,256,1024]{2,1,0:T(8,128)(2,1)}, bf16[2,256,1024]{2,1,0:T(8,128)(2,1)S(1)}, u32[]{:S(2)}, u32[]{:S(2)}) collective-permute-start(bf16[2,256,1024]{2,1,0:T(8,128)(2,1)} %collective-permute-done.13.refs_0_), channel_id=1, source_target_pairs={{0,1},{1,0},{2,3},{3,2},{4,5},{5,4},{6,7},{7,6},{8,9},{9,8},{10,11... | collective-permute-start | bytes 3145736 | tf_op jit(solution)/shard_map/ppermute | solution.py:265
  589.9 26.6 %collective-permute-start.16 = (bf16[2,256,1024]{2,1,0:T(8,128)(2,1)S(1)}, bf16[2,256,1024]{2,1,0:T(8,128)(2,1)S(1)}, u32[]{:S(2)}, u32[]{:S(2)}) collective-permute-start(bf16[2,256,1024]{2,1,0:T(8,128)(2,1)S(1)} %collective-permute-done.14.refs_1_), channel_id=1, source_target_pairs={{0,1},{1,0},{2,3},{3,2},{4,5},{5,4},{6,7},{7,6},{8,9},{9,8},{10,11... | collective-permute-start | bytes 3145736 | tf_op jit(solution)/shard_map/ppermute | solution.py:265
  590.8 26.0 %collective-permute-start.19 = (bf16[2,256,1024]{2,1,0:T(8,128)(2,1)}, bf16[2,256,1024]{2,1,0:T(8,128)(2,1)}, u32[]{:S(2)}, u32[]{:S(2)}) collective-permute-start(bf16[2,256,1024]{2,1,0:T(8,128)(2,1)} %collective-permute-done.17.refs_4_), channel_id=1, source_target_pairs={{0,1},{1,0},{2,3},{3,2},{4,5},{5,4},{6,7},{7,6},{8,9},{9,8},{10,11... | collective-permute-start | bytes 3145736 | tf_op jit(solution)/shard_map/ppermute | solution.py:265
  590.9 26.1 %collective-permute-start.20 = (bf16[2,256,1024]{2,1,0:T(8,128)(2,1)}, bf16[2,256,1024]{2,1,0:T(8,128)(2,1)}, u32[]{:S(2)}, u32[]{:S(2)}) collective-permute-start(bf16[2,256,1024]{2,1,0:T(8,128)(2,1)} %collective-permute-done.18.refs_5_), channel_id=1, source_target_pairs={{0,1},{1,0},{2,3},{3,2},{4,5},{5,4},{6,7},{7,6},{8,9},{9,8},{10,11... | collective-permute-start | bytes 3145736 | tf_op jit(solution)/shard_map/ppermute | solution.py:265
  615.8 43.0 %collective-permute-start.11 = (bf16[1024,512]{1,0:T(8,128)(2,1)}, bf16[1024,512]{1,0:T(8,128)(2,1)}, u32[]{:S(2)}, u32[]{:S(2)}) collective-permute-start(bf16[1024,512]{1,0:T(8,128)(2,1)} %collective-permute-done.10.refs_10_), channel_id=1, source_target_pairs={{0,1},{1,0},{2,3},{3,2},{4,5},{5,4},{6,7},{7,6},{8,9},{9,8},{10,11... | collective-permute-start | bytes 3145736 | tf_op jit(solution)/shard_map/ppermute | solution.py:265
  616.2 42.7 %collective-permute-start.3 = (bf16[2,256,1024]{2,1,0:T(8,128)(2,1)S(1)}, bf16[2,256,1024]{2,1,0:T(8,128)(2,1)}, u32[]{:S(2)}, u32[]{:S(2)}) collective-permute-start(bf16[2,256,1024]{2,1,0:T(8,128)(2,1)S(1)} %collective-permute-done.1.refs_0_), channel_id=1, source_target_pairs={{0,1},{1,0},{2,3},{3,2},{4,5},{5,4},{6,7},{7,6},{8,9},{9,8},{10,11... | collective-permute-start | bytes 3145736 | tf_op jit(solution)/shard_map/ppermute | solution.py:265
  616.5 42.4 %collective-permute-start.4 = (bf16[2,256,1024]{2,1,0:T(8,128)(2,1)S(1)}, bf16[2,256,1024]{2,1,0:T(8,128)(2,1)S(1)}, u32[]{:S(2)}, u32[]{:S(2)}) collective-permute-start(bf16[2,256,1024]{2,1,0:T(8,128)(2,1)S(1)} %collective-permute-done.2.refs_1_), channel_id=1, source_target_pairs={{0,1},{1,0},{2,3},{3,2},{4,5},{5,4},{6,7},{7,6},{8,9},{9,8},{10,11... | collective-permute-start | bytes 3145736 | tf_op jit(solution)/shard_map/ppermute | solution.py:265
  616.8 42.0 %collective-permute-start.7 = (bf16[2,256,1024]{2,1,0:T(8,128)(2,1)S(1)}, bf16[2,256,1024]{2,1,0:T(8,128)(2,1)}, u32[]{:S(2)}, u32[]{:S(2)}) collective-permute-start(bf16[2,256,1024]{2,1,0:T(8,128)(2,1)S(1)} %collective-permute-done.5.refs_4_), channel_id=1, source_target_pairs={{0,1},{1,0},{2,3},{3,2},{4,5},{5,4},{6,7},{7,6},{8,9},{9,8},{10,11... | collective-permute-start | bytes 3145736 | tf_op jit(solution)/shard_map/ppermute | solution.py:265
  617.1 41.8 %collective-permute-start.8 = (bf16[2,256,1024]{2,1,0:T(8,128)(2,1)S(1)}, bf16[2,256,1024]{2,1,0:T(8,128)(2,1)}, u32[]{:S(2)}, u32[]{:S(2)}) collective-permute-start(bf16[2,256,1024]{2,1,0:T(8,128)(2,1)S(1)} %copy-done.10), channel_id=1, source_target_pairs={{0,1},{1,0},{2,3},{3,2},{4,5},{5,4},{6,7},{7,6},{8,9},{9,8},{10,11... | collective-permute-start | bytes 3145736 | tf_op jit(solution)/shard_map/ppermute | solution.py:265
  680.2 11.5 %collective-permute-start.56 = (bf16[96,2048]{1,0:T(8,128)(2,1)}, bf16[96,2048]{1,0:T(8,128)(2,1)S(1)}, u32[]{:S(2)}, u32[]{:S(2)}) collective-permute-start(bf16[96,2048]{1,0:T(8,128)(2,1)} %get-tuple-element.79), channel_id=1, source_target_pairs={{0,4},{1,5},{2,6},{3,7},{4,0},{5,1},{6,2},{7,3},{8,12},{9,13},{10,... | collective-permute-start | bytes 1179656 | tf_op jit(solution)/shard_map/ppermute | solution.py:265
  680.9 29.1 %collective-permute-start.57 = (bf16[96,2048]{1,0:T(8,128)(2,1)}, bf16[96,2048]{1,0:T(8,128)(2,1)S(1)}, u32[]{:S(2)}, u32[]{:S(2)}) collective-permute-start(bf16[96,2048]{1,0:T(8,128)(2,1)} %get-tuple-element.80), channel_id=1, source_target_pairs={{0,8},{1,9},{2,10},{3,11},{4,12},{5,13},{6,14},{7,15},{8,0},{9,1},... | collective-permute-start | bytes 1179656 | tf_op jit(solution)/shard_map/ppermute | solution.py:265
  687.4 30.0 %collective-permute-start.58 = (bf16[96,2048]{1,0:T(8,128)(2,1)}, bf16[96,2048]{1,0:T(8,128)(2,1)S(1)}, u32[]{:S(2)}, u32[]{:S(2)}) collective-permute-start(bf16[96,2048]{1,0:T(8,128)(2,1)} %get-tuple-element.81), channel_id=1, source_target_pairs={{0,12},{1,13},{2,14},{3,15},{4,8},{5,9},{6,10},{7,11},{8,4},{9,5},... | collective-permute-start | bytes 1179656 | tf_op jit(solution)/shard_map/ppermute | solution.py:265
  687.7 29.7 %collective-permute-start.59 = (bf16[96,2048]{1,0:T(8,128)(2,1)}, bf16[96,2048]{1,0:T(8,128)(2,1)S(1)}, u32[]{:S(2)}, u32[]{:S(2)}) collective-permute-start(bf16[96,2048]{1,0:T(8,128)(2,1)} %get-tuple-element.82), channel_id=1, source_target_pairs={{0,16},{1,17},{2,18},{3,19},{4,20},{5,21},{6,22},{7,23},{8,24},{9,... | collective-permute-start | bytes 1179656 | tf_op jit(solution)/shard_map/ppermute | solution.py:265
  687.7 52.0 %collective-permute-start.60 = (bf16[96,2048]{1,0:T(8,128)(2,1)}, bf16[96,2048]{1,0:T(8,128)(2,1)S(1)}, u32[]{:S(2)}, u32[]{:S(2)}) collective-permute-start(bf16[96,2048]{1,0:T(8,128)(2,1)} %get-tuple-element.83), channel_id=1, source_target_pairs={{0,20},{1,21},{2,22},{3,23},{4,16},{5,17},{6,18},{7,19},{8,28},{9,... | collective-permute-start | bytes 1179656 | tf_op jit(solution)/shard_map/ppermute | solution.py:265
  691.7 60.3 %collective-permute-start.61 = (bf16[96,2048]{1,0:T(8,128)(2,1)}, bf16[96,2048]{1,0:T(8,128)(2,1)S(1)}, u32[]{:S(2)}, u32[]{:S(2)}) collective-permute-start(bf16[96,2048]{1,0:T(8,128)(2,1)} %get-tuple-element.84), channel_id=1, source_target_pairs={{0,24},{1,25},{2,26},{3,27},{4,28},{5,29},{6,30},{7,31},{8,16},{9,... | collective-permute-start | bytes 1179656 | tf_op jit(solution)/shard_map/ppermute | solution.py:265
  710.0 49.5 %collective-permute-start.62 = (bf16[96,2048]{1,0:T(8,128)(2,1)}, bf16[96,2048]{1,0:T(8,128)(2,1)S(1)}, u32[]{:S(2)}, u32[]{:S(2)}) collective-permute-start(bf16[96,2048]{1,0:T(8,128)(2,1)} %get-tuple-element.85), channel_id=1, source_target_pairs={{0,28},{1,29},{2,30},{3,31},{4,24},{5,25},{6,26},{7,27},{8,20},{9,... | collective-permute-start | bytes 1179656 | tf_op jit(solution)/shard_map/ppermute | solution.py:265
  (21 other events, 1541.7 us)
